TPU v7x, 32 devices: a whole 2x2x4 slice. The times are simulated.
32 devices in a mesh: grp: 2 (over y), sp: 4 (over z), tp: 4 (over x, core).
Axes of the slice: x: 2, y: 2, z: 4, core: 2. Of those that a mesh axis runs over, the one named last changes fastest.
Arguments:
- queries: bfloat16 [6144, 512], P(('grp', 'sp'), 'tp'), parts along dimension 0, may hold values from -6 to 6
- key_projected: bfloat16 [6144, 512], P(('grp', 'sp'), 'tp'), parts along dimension 0, may hold values from -6 to 6
- values: bfloat16 [6144, 1024], P(('grp', 'sp'), 'tp'), parts along dimension 0, may hold values from -6 to 6
- output_gate_preact: bfloat16 [6144, 1024], P(('grp', 'sp'), 'tp'), parts along dimension 0, may hold values from -6 to 6
- forward_decay_logits: bfloat16 [6144, 512], P(('grp', 'sp'), 'tp'), parts along dimension 0, may hold values from -3.8 to 3.8
- backward_decay_logits: bfloat16 [6144, 512], P(('grp', 'sp'), 'tp'), parts along dimension 0, may hold values from -3.8 to 3.8
- decay_logit_shift: float32 [2, 512], P(None, 'tp'), may hold values from -1 to 13
- decay_spike_values: float32 [8, 6144], P('tp', ('grp', 'sp')), parts along dimension 1, may hold values from -2.1 to 0
- residual: bfloat16 [6144, 2048], P(('grp', 'sp', 'tp')), parts along dimension 0, may hold values from -6 to 6
- head_norm_gain: float32 [1024], P('tp'), may hold values from 0.1 to 1.9
- output_projection: bfloat16 [1024, 2048], P('tp'), may hold values from -0.1875 to 0.1875
- prenorm_gain: float32 [2048], replicated, may hold values from 0.1 to 1.9
- gate_projection: bfloat16 [2048, 5120], P('sp', 'tp'), may hold values from -0.125 to 0.125
- up_projection: bfloat16 [2048, 5120], P('sp', 'tp'), may hold values from -0.125 to 0.125
- down_projection: bfloat16 [5120, 2048], P('tp', 'sp'), may hold values from -0.078125 to 0.078125
Outputs:
- layer_output: bfloat16 [6144, 2048], P(('grp', 'sp', 'tp')), parts along dimension 0
There are 2 independent parts, one for each index of `grp`. A program takes and returns all parts, laid end to end along the dimension named above; an argument that names none is the same for every part. Nothing has to cross between parts.
All inputs are finite; a program needn't handle non-finite values.
Results may differ from a plain program's by a relative error of at most 0.014.
Values may be sent and summed in bfloat16 or wider, within the bound.
A program may use at most 64 MiB of HBM per device.

v0:
```python
import jax
import jax.numpy as jnp
from jax import lax
from jax.sharding import PartitionSpec as P

KEY_CHANNELS = 64
HEAD_V = 128
BLOCK = 64
gate_denominator = 16.0
norm_epsilon = 1e-06


def entering(value, axis, join, neutral, backward):
    count = lax.axis_size(axis)
    place = lax.axis_index(axis)
    ahead = count - 1 - place if backward else place
    gathered = jax.tree.map(
        lambda a, kind: lax.all_gather(a.astype(kind), axis), value, (jnp.bfloat16, jnp.bfloat16)
    )
    state = jax.tree.map(lambda a, e: jnp.zeros_like(a) + jnp.asarray(e, a.dtype), value, neutral)

    def one(lap, state):
        source = count - 1 - lap if backward else lap
        return join(
            state,
            jax.tree.map(
                lambda a, own: lax.dynamic_index_in_dim(a, source, 0, False).astype(own.dtype),
                gathered,
                value,
            ),
        )

    return lax.fori_loop(0, ahead, one, state)


def block_sweep(query_in, key_in, values_in, log_decay, span):
    sequence_length, head_count, key_dim = key_in.shape
    block_count = sequence_length // span

    def blocks(tensor):
        return jnp.transpose(
            tensor.reshape(block_count, span, head_count, tensor.shape[-1]), (0, 2, 1, 3)
        )

    lower_mask = jnp.tril(jnp.ones((span, span), dtype=bool))[:, :, None]

    def advance(carried, inputs):
        memory, offset = carried
        key_blk, value_blk, decay_blk, query_blk = inputs
        within = jnp.cumsum(decay_blk, axis=1)
        ending = within[:, -1, :]
        memory_next = jnp.exp(ending)[:, :, None] * memory + jnp.einsum(
            "hjd,hje->hde",
            key_blk * jnp.exp(ending[:, None, :] - within),
            value_blk,
            precision=lax.Precision.HIGHEST,
        )
        result = jnp.einsum(
            "hid,hde->hie", query_blk * jnp.exp(within), memory, precision=lax.Precision.HIGHEST
        )
        spread = jnp.exp(
            jnp.where(lower_mask, within[:, :, None, :] - within[:, None, :, :], -jnp.inf)
        )
        scores = jnp.einsum(
            "hid,hjd,hijd->hij", query_blk, key_blk, spread, precision=lax.Precision.HIGHEST
        )
        result = result + jnp.einsum(
            "hij,hje->hie", scores, value_blk, precision=lax.Precision.HIGHEST
        )
        reached = query_blk * jnp.exp(within + offset[:, None, :])
        return ((memory_next, offset + ending), (result, reached))

    start_memory = jnp.zeros((head_count, key_dim, values_in.shape[-1]), jnp.float32)
    start_offset = jnp.zeros((head_count, key_dim), jnp.float32)
    (memory, decay_total), (outputs, reached) = lax.scan(
        advance,
        (start_memory, start_offset),
        (blocks(key_in), blocks(values_in), blocks(log_decay), blocks(query_in)),
    )

    def unblock(tensor):
        return jnp.transpose(tensor, (0, 2, 1, 3)).reshape(
            sequence_length, head_count, tensor.shape[-1]
        )

    return (unblock(outputs), unblock(reached), memory, decay_total)


def head_mix(combined, head_norm_gain, output_gate_preact):
    sequence_length, head_count, width = combined.shape
    inverse = lax.rsqrt(jnp.mean(combined * combined, axis=-1, keepdims=True) + norm_epsilon)
    gate_act = jax.nn.silu(
        output_gate_preact.astype(jnp.float32).reshape(sequence_length, head_count, width)
    )
    weighted = combined * inverse * head_norm_gain.reshape(head_count, width) * gate_act
    return weighted.reshape(sequence_length, head_count * width).astype(jnp.bfloat16)


def row_norm(mid_rows, prenorm_gain):
    wide = mid_rows.astype(jnp.float32)
    inverse = lax.rsqrt(jnp.mean(wide * wide, axis=-1, keepdims=True) + norm_epsilon)
    return (wide * inverse * prenorm_gain).astype(jnp.bfloat16)


def combine_states(earlier, later):
    decay_early, memory_early = earlier
    decay_late, memory_late = later
    return (decay_early * decay_late, decay_late[:, :, None] * memory_early + memory_late)


def body(
    queries,
    key_projected,
    values,
    output_gate_preact,
    forward_decay_logits,
    backward_decay_logits,
    decay_logit_shift,
    decay_spike_values,
    residual,
    head_norm_gain,
    output_projection,
    prenorm_gain,
    gate_projection,
    up_projection,
    down_projection,
):
    sequence_length = queries.shape[0]
    local_heads = queries.shape[1] // KEY_CHANNELS
    query_f = queries.astype(jnp.float32).reshape(
        sequence_length, local_heads, KEY_CHANNELS
    ) * KEY_CHANNELS ** (-0.5)
    keys_f = key_projected.astype(jnp.float32).reshape(sequence_length, local_heads, KEY_CHANNELS)
    values_f = values.astype(jnp.float32).reshape(sequence_length, local_heads, HEAD_V)
    decay_spikes = jnp.transpose(decay_spike_values)[:, :, None]
    logit_shifts = decay_logit_shift.reshape(2, local_heads, KEY_CHANNELS)
    forward_decay = (
        jax.nn.log_sigmoid(
            forward_decay_logits.astype(jnp.float32).reshape(
                sequence_length, local_heads, KEY_CHANNELS
            )
            + logit_shifts[0]
        )
        / gate_denominator
        + decay_spikes
    )
    backward_decay = (
        jax.nn.log_sigmoid(
            backward_decay_logits.astype(jnp.float32).reshape(
                sequence_length, local_heads, KEY_CHANNELS
            )
            + logit_shifts[1]
        )
        / gate_denominator
        + decay_spikes
    )
    fwd_out, fwd_reach, fwd_memory, fwd_total = block_sweep(
        query_f, keys_f, values_f, forward_decay, BLOCK
    )
    bwd_out, bwd_reach, bwd_memory, bwd_total = block_sweep(
        query_f[::-1], keys_f[::-1], values_f[::-1], backward_decay[::-1], BLOCK
    )
    identity = (jnp.ones_like(fwd_total), jnp.zeros_like(fwd_memory))
    fwd_incoming = entering(
        (jnp.exp(fwd_total), fwd_memory), "sp", combine_states, identity, False
    )[1]
    bwd_incoming = entering((jnp.exp(bwd_total), bwd_memory), "sp", combine_states, identity, True)[
        1
    ]
    fwd_full = fwd_out + jnp.einsum(
        "lhd,hde->lhe", fwd_reach, fwd_incoming, precision=lax.Precision.HIGHEST
    )
    bwd_full = bwd_out + jnp.einsum(
        "lhd,hde->lhe", bwd_reach, bwd_incoming, precision=lax.Precision.HIGHEST
    )
    attended = head_mix(fwd_full + bwd_full[::-1], head_norm_gain, output_gate_preact)
    token_rows = lax.all_to_all(attended, "tp", split_axis=0, concat_axis=1, tiled=True)
    whole_out = lax.all_gather(output_projection, "tp", axis=0, tiled=True)
    projected = jnp.dot(token_rows, whole_out, preferred_element_type=jnp.float32)
    mid_rows = (residual.astype(jnp.float32) + projected).astype(jnp.bfloat16)
    normed = row_norm(mid_rows, prenorm_gain)
    fetched = (
        lax.all_gather(gate_projection, "sp", axis=0, tiled=True),
        lax.all_gather(up_projection, "sp", axis=0, tiled=True),
        lax.all_gather(down_projection, "sp", axis=1, tiled=True),
    )
    gate_full, up_full, down_full = fetched
    piece = lax.all_gather(normed, "tp", axis=0, tiled=True)
    gate_part = jnp.dot(piece, gate_full, preferred_element_type=jnp.float32)
    up_part = jnp.dot(piece, up_full, preferred_element_type=jnp.float32)
    hidden = (jax.nn.silu(gate_part) * up_part).astype(jnp.bfloat16)
    summed = lax.psum_scatter(
        jnp.dot(hidden, down_full, preferred_element_type=jnp.float32).astype(jnp.bfloat16),
        "tp",
        scatter_dimension=0,
        tiled=True,
    ).astype(jnp.float32)
    return (mid_rows.astype(jnp.float32) + 0.5 * summed).astype(jnp.bfloat16)


def solution(mesh):
    in_specs = (
        P(("grp", "sp"), "tp"),
        P(("grp", "sp"), "tp"),
        P(("grp", "sp"), "tp"),
        P(("grp", "sp"), "tp"),
        P(("grp", "sp"), "tp"),
        P(("grp", "sp"), "tp"),
        P(None, "tp"),
        P("tp", ("grp", "sp")),
        P(("grp", "sp", "tp"), None),
        P("tp"),
        P("tp", None),
        P(),
        P("sp", "tp"),
        P("sp", "tp"),
        P("tp", "sp"),
    )
    out_specs = P(("grp", "sp", "tp"), None)
    return jax.shard_map(body, mesh=mesh, in_specs=in_specs, out_specs=out_specs, check_vma=False)
```

profile of v0, /device:TPU:0, one launch (start us, length us, event | category | flops | bytes accessed | tf_op | source)
XLA Modules:
  0.0 782.6 jit_solution(11281532606499490096)
XLA Ops:
  31.3 173.5 %while.62 = (s32[]{:T(128)}, f32[2,64,128]{2,1,0:T(8,128)S(1)}, f32[2,64]{1,0:T(2,128)S(1)}, f32[12,2,64,128]{3,2,0,1:T(8,128)S(1)}, f32[12,2,64,64]{3,2,1,0:T(8...) while((s32[]{:T(128)}, f32[2,64,128]{2,1,0:T(8,128)S(1)}, ...), condition=%wide.region_2.3_spmd.clone, body=%wide.region_0.2_spmd.clone.sunk | while | flops 41005312 | bytes 10040985 | solution.py:75
  34.4 5.6 copy.189
  45.8 3.0 select_exponential_fusion.4
  48.8 5.6 copy.189
  55.5 3.2 fusion.109
  60.6 3.0 select_exponential_fusion.4
  63.6 5.6 copy.189
  78.1 5.6 copy.189
  92.5 5.6 copy.189
  104.0 3.0 select_exponential_fusion.4
  107.0 5.6 copy.189
  121.4 5.6 copy.189
  132.9 3.0 select_exponential_fusion.4
  135.8 5.6 copy.189
  150.3 5.6 copy.189
  161.7 3.0 select_exponential_fusion.4
  164.7 5.6 copy.189
  179.1 5.6 copy.189
  193.5 5.6 copy.189
  205.8 209.2 %while.63 = (s32[]{:T(128)}, f32[2,64,128]{2,1,0:T(8,128)S(1)}, f32[2,64]{1,0:T(2,128)S(1)}, f32[12,2,64,128]{3,2,0,1:T(8,128)S(1)}, f32[12,2,64,64]{3,2,1,0:T(8...) while((s32[]{:T(128)}, f32[2,64,128]{2,1,0:T(8,128)S(1)}, ...), condition=%wide.region_7.8_spmd.clone, body=%wide.region_5.7_spmd.clone.sunk | while | flops 41005312 | bytes 9845901 | solution.py:75
  210.1 5.6 copy.195
  227.5 5.6 copy.195
  245.0 5.6 copy.195
  262.4 5.6 copy.195
  279.8 5.6 copy.195
  297.3 5.6 copy.195
  311.7 3.0 select_exponential_fusion.5
  314.7 5.6 copy.195
  332.1 5.6 copy.195
  349.6 5.6 copy.195
  364.0 3.0 select_exponential_fusion.5
  367.0 5.6 copy.195
  381.5 3.0 select_exponential_fusion.5
  384.4 5.6 copy.195
  401.9 5.6 copy.195
  419.2 12.9 %all-gather.5 = bf16[4,2,64]{2,1,0:T(2,128)(2,1)S(1)} all-gather(bf16[1,2,64]{2,1,0:T(2,128)(2,1)S(1)} %fusion.66), channel_id=4, replica_groups=mesh['grp'=2,'sp'=4,'tp'=4] {'sp'}, dimensions={0}, use_global_device_ids=true | all-gather | bytes 1280 | tf_op jit(solution)/shard_map/all_gather | solution.py:18
  432.1 13.4 %all-gather.3 = bf16[8,64,128]{2,1,0:T(8,128)(2,1)S(1)} all-gather(bf16[2,64,128]{2,1,0:T(8,128)(2,1)S(1)} %convert_element_type.105), channel_id=5, replica_groups=mesh['grp'=2,'sp'=4,'tp'=4] {'sp'}, dimensions={0}, use_global_device_ids=true | all-gather | bytes 163840 | tf_op jit(solution)/shard_map/all_gather | solution.py:18
  447.8 7.3 rev.19
  457.3 7.6 all-gather.4
  464.9 13.3 %all-gather.1 = bf16[8,64,128]{2,1,0:T(8,128)(2,1)S(1)} all-gather(bf16[2,64,128]{2,1,0:T(8,128)(2,1)S(1)} %convert_element_type.103), channel_id=3, replica_groups=mesh['grp'=2,'sp'=4,'tp'=4] {'sp'}, dimensions={0}, use_global_device_ids=true | all-gather | bytes 163840 | tf_op jit(solution)/shard_map/all_gather | solution.py:18
  481.3 10.0 %all_to_all.16 = bf16[4,192,256]{2,1,0:T(8,128)(2,1)S(1)} all-to-all(bf16[4,192,256]{2,1,0:T(8,128)(2,1)S(1)} %convert_element_type.107), channel_id=1, replica_groups=mesh['grp'=2,'sp'=4,'tp'=4] {'tp'}, dimensions={0} | all-to-all | bytes 786432 | tf_op jit(solution)/shard_map/all_to_all | solution.py:177
  491.3 3.5 multiply_reduce_fusion
  497.2 26.7 %all-gather.14.cloned.1.call-done = bf16[768,2048]{1,0:T(8,128)(2,1)} async-done(((bf16[192,2048]{1,0:T(8,128)(2,1)}), bf16[768,2048]{1,0:T(8,128)(2,1)}) %all-gather.14.cloned.1.call-update) | async-done | bytes 3145744 | tf_op jit(solution)/shard_map/all_gather | solution.py:188
  523.9 9.6 %fusion.70 = f32[768,1280]{1,0:T(8,128)} fusion(bf16[768,2048]{1,0:T(8,128)(2,1)} %all-gather.14.cloned.1.call-done, bf16[2048,1280]{1,0:T(8,128)(2,1)} %all-gather.16.cloned.1.call-done), kind=kOutput, calls=%fused_computation.119 | convolution fusion | flops 4026531840 | bytes 12320768 | tf_op jit(solution)/shard_map/dot_general | solution.py:189
  533.4 89.9 %all-gather.18.cloned.1.call-done = bf16[2048,1280]{1,0:T(8,128)(2,1)} async-done(((bf16[512,1280]{1,0:T(8,128)(2,1)}), bf16[2048,1280]{1,0:T(8,128)(2,1)}) %all-gather.18.cloned.1.call-update) | async-done | bytes 5242896 | tf_op jit(solution)/shard_map/all_gather | solution.py:184
  623.4 97.8 %all-gather.20.cloned.1.call-done = bf16[1280,2048]{1,0:T(8,128)(2,1)} async-done(((bf16[1280,512]{1,0:T(8,128)(2,1)}), bf16[1280,2048]{1,0:T(8,128)(2,1)}) %all-gather.20.cloned.1.call-update) | async-done | bytes 5242896 | tf_op jit(solution)/shard_map/all_gather | solution.py:185
  721.2 16.0 %convolution_convert_fusion = bf16[768,2048]{1,0:T(8,128)(2,1)} fusion(bf16[1280,2048]{1,0:T(8,128)(2,1)} %all-gather.20.cloned.1.call-done, bf16[768,2048]{1,0:T(8,128)(2,1)} %all-gather.14.cloned.1.call-done, bf16[2048,1280]{1,0:T(8,128)(2,1)} %all-gather.18.cloned.1.call-done, f32[768,1280]{1,0:T(8,128)} %fusion.70), kind=kOutput, calls=%fused_computation.75 | convolution fusion | flops 8060534784 | bytes 20709376 | tf_op jit(solution)/shard_map/dot_general | solution.py:193
  737.2 36.4 %reduce-scatter.2.cloned.1.call-done = bf16[192,2048]{1,0:T(8,128)(2,1)} async-done(((bf16[768,2048]{1,0:T(8,128)(2,1)}), bf16[192,2048]{1,0:T(8,128)(2,1)}) %reduce-scatter.2.cloned.1.call-update) | async-done | bytes 786448 | tf_op jit(solution)/shard_map/reduce_scatter | solution.py:192
  (465 shorter events, 261.1 us)
Async XLA Ops:
  6.5 3.0 copy-start.3
  6.5 4.8 copy-start.9
  6.5 4.9 copy-start.4
  6.5 5.0 copy-start.6
  6.5 484.8 %all-gather.12.cloned.1.call-start = ((), (), s32[]{:S(2)}) async-start(), calls=%async_computation.2 | async-start | bytes 5242880 | tf_op jit(solution)/shard_map/all_gather | solution.py:178
  7.3 489.9 %all-gather.16.cloned.1.call-start = ((), (), s32[]{:S(2)}) async-start(), calls=%async_computation.4 | async-start | bytes 6553600 | tf_op jit(solution)/shard_map/all_gather | solution.py:183
  8.0 515.9 %all-gather.14.cloned.1.call-start = ((), (), s32[]{:S(2)}) async-start(), calls=%async_computation.3 | async-start | bytes 3932160 | tf_op jit(solution)/shard_map/all_gather | solution.py:188
  11.8 8.5 %copy-start.5 = (bf16[768,128]{1,0:T(8,128)(2,1)S(1)}, bf16[768,128]{1,0:T(8,128)(2,1)}, u32[]{:S(2)}) copy-start(bf16[768,128]{1,0:T(8,128)(2,1)} %param.23) | copy-start | bytes 589828
  415.0 0.9 copy-start
  447.8 9.3 %copy-start.2 = (bf16[768,256]{1,0:T(8,128)(2,1)S(1)}, bf16[768,256]{1,0:T(8,128)(2,1)}, u32[]{:S(2)}) copy-start(bf16[768,256]{1,0:T(8,128)(2,1)} %param.26) | copy-start | bytes 1179652
  455.6 22.6 %copy-start.1 = (f32[768,2,128]{0,2,1:T(8,128)S(1)}, f32[768,2,128]{0,2,1:T(8,128)}, u32[]{:S(2)}) copy-start(f32[768,2,128]{0,2,1:T(8,128)} %rev.19) | copy-start | bytes 2359300
  455.7 24.6 %copy-start.8 = (f32[256]{0:T(256)S(1)}, f32[256]{0:T(256)}, u32[]{:S(2)}) copy-start(f32[256]{0:T(256)} %param.32) | copy-start | bytes 3076
  481.3 13.6 %copy-start.7 = (f32[2048]{0:T(1024)S(1)}, f32[2048]{0:T(1024)}, u32[]{:S(2)}) copy-start(f32[2048]{0:T(1024)} %param.34) | copy-start | bytes 24580
  496.0 127.4 %all-gather.18.cloned.1.call-start = ((), (), s32[]{:S(2)}) async-start(), calls=%async_computation.5 | async-start | bytes 6553600 | tf_op jit(solution)/shard_map/all_gather | solution.py:184
  496.6 224.6 %all-gather.20.cloned.1.call-start = ((), (), s32[]{:S(2)}) async-start(), calls=%async_computation.6 | async-start | bytes 6553600 | tf_op jit(solution)/shard_map/all_gather | solution.py:185
  497.1 276.4 %reduce-scatter.2.cloned.1.call-start = ((), (), s32[]{:S(2)}) async-start(), calls=%async_computation.7 | async-start | bytes 3932160 | tf_op jit(solution)/shard_map/reduce_scatter | solution.py:192
Sparse Core Ops, SparseCore 0:
  8.9 37.1 all-gather.11
  47.7 98.0 all-gather.15
  496.1 27.7 all-gather.13
  525.3 98.0 all-gather.17
  624.8 96.3 all-gather.19
  737.3 36.1 reduce-scatter.1
where the time goes:
time: 788 us; the launch traced here: 783 us
  waiting for transfers between devices  253 us (32%)
  local copies, waits for them, and re-layouts  224 us (28%)
  other arithmetic  159 us (20%)
  matrix products  72.5 us (9%)
  blocking collectives  57.2 us (7%)
  between operations  13.9 us (2%)
    while x24, local copies, waits for them, and re-layouts  134 us
    all_gather x1, waiting for transfers between devices, body(): lax.all_gather(down_projection, 'sp', axis=1, tiled=True)  97.8 us
    all_gather x1, waiting for transfers between devices, body(): lax.all_gather(up_projection, 'sp', axis=0, tiled=True)  89.9 us
    exp x24, other arithmetic, advance(): jnp.exp(jnp.where(lower_mask, within[:, :, None, :] - within[:, None, :,...  71.7 us
    dot_general x24, other arithmetic, advance(): jnp.einsum('hid,hjd,hijd->hij', query_blk, key_blk, spread, precision=lax...  69 us
    dynamic_slice x108, local copies, waits for them, and re-layouts, block_sweep(): lax.scan(advance, (start_memory, start_offset), (blocks(key_in), blocks(v...  52.5 us
    all_gather x4, blocking collectives, entering(): lax.all_gather(a.astype(kind), axis)  47.2 us
    reduce_scatter x1, waiting for transfers between devices, body(): lax.psum_scatter(jnp.dot(hidden, down_full, preferred_element_type=jnp.fl...  36.4 us
  transfers between devices with their start and end apart: 6, of which 4 were waited for; matrix products, arithmetic and copies ran while one was open for 56% of the time, Pallas kernels for 0%

commit v1 on v0

--- a/solution.py
+++ b/solution.py
@@ -182,7 +182,7 @@
     fetched = (
         lax.all_gather(gate_projection, "sp", axis=0, tiled=True),
         lax.all_gather(up_projection, "sp", axis=0, tiled=True),
-        lax.all_gather(down_projection, "sp", axis=1, tiled=True),
+        jnp.concatenate(jax.lax.all_gather(down_projection, axis_name="sp"), 1),
     )
     gate_full, up_full, down_full = fetched
     piece = lax.all_gather(normed, "tp", axis=0, tiled=True)

time: 788 us -> 691 us (0.88)
  waiting for transfers between devices: 253 us -> 148 us
  local copies, waits for them, and re-layouts: 224 us -> 232 us
    all_gather x1, waiting for transfers between devices: 97.8 us -> 0.02 us  [body(): jax.lax.all_gather(down_projection, axis_name='sp')]
    reshape x0 -> x1, local copies, waits for them, and re-layouts: none -> 7.98 us  [body(): jnp.concatenate(jax.lax.all_gather(down_projection, axis_name='sp'), 1)]
  transfers between devices with their start and end apart: 6 -> 6, of which waited for: 4 -> 3; matrix products, arithmetic and copies ran while one was open for 56% -> 65% of each run, Pallas kernels for 0% -> 0%
where the time goes in v1:
time: 691 us; the launch traced here: 686 us
  local copies, waits for them, and re-layouts  232 us (34%)
  other arithmetic  159 us (23%)
  waiting for transfers between devices  148 us (21%)
  matrix products  72.5 us (10%)
  blocking collectives  57 us (8%)
  between operations  13.8 us (2%)
    while x24, local copies, waits for them, and re-layouts  135 us
    all_gather x1, waiting for transfers between devices, body(): lax.all_gather(up_projection, 'sp', axis=0, tiled=True)  89.9 us
    exp x24, other arithmetic, advance(): jnp.exp(jnp.where(lower_mask, within[:, :, None, :] - within[:, None, :,...  71.7 us
    dot_general x24, other arithmetic, advance(): jnp.einsum('hid,hjd,hijd->hij', query_blk, key_blk, spread, precision=lax...  69 us
    dynamic_slice x108, local copies, waits for them, and re-layouts, block_sweep(): lax.scan(advance, (start_memory, start_offset), (blocks(key_in), blocks(v...  52.5 us
    all_gather x4, blocking collectives, entering(): lax.all_gather(a.astype(kind), axis)  47.1 us
    reduce_scatter x1, waiting for transfers between devices, body(): lax.psum_scatter(jnp.dot(hidden, down_full, preferred_element_type=jnp.fl...  36.4 us
    all_gather x1, waiting for transfers between devices, body(): piece = lax.all_gather(normed, 'tp', axis=0, tiled=True)  19.2 us
  transfers between devices with their start and end apart: 6, of which 3 were waited for; matrix products, arithmetic and copies ran while one was open for 65% of the time, Pallas kernels for 0%

profile of v1, /device:TPU:0, one launch (start us, length us, event | category | flops | bytes accessed | tf_op | source)
XLA Modules:
  0.0 685.6 jit_solution(13901278364404752746)
XLA Ops:
  32.0 173.7 %while.62 = (s32[]{:T(128)}, f32[2,64,128]{2,1,0:T(8,128)S(1)}, f32[2,64]{1,0:T(2,128)S(1)}, f32[12,2,64,128]{3,2,0,1:T(8,128)S(1)}, f32[12,2,64,64]{3,2,1,0:T(8...) while((s32[]{:T(128)}, f32[2,64,128]{2,1,0:T(8,128)S(1)}, ...), condition=%wide.region_2.3_spmd.clone, body=%wide.region_0.2_spmd.clone.sunk | while | flops 41005312 | bytes 10040985 | solution.py:75
  32.2 3.0 select_exponential_fusion.4
  35.2 5.6 copy.191
  46.6 3.0 select_exponential_fusion.4
  49.6 5.6 copy.191
  56.3 3.2 fusion.109
  61.4 3.0 select_exponential_fusion.4
  64.4 5.6 copy.191
  75.8 3.0 select_exponential_fusion.4
  78.8 5.6 copy.191
  90.3 3.0 select_exponential_fusion.4
  93.3 5.6 copy.191
  104.7 3.0 select_exponential_fusion.4
  107.7 5.6 copy.191
  119.1 3.0 select_exponential_fusion.4
  122.1 5.6 copy.191
  133.5 3.0 select_exponential_fusion.4
  136.5 5.6 copy.191
  150.9 5.8 copy.191
  165.6 5.6 copy.191
  180.0 5.6 copy.191
  194.5 5.6 copy.191
  206.8 209.1 %while.63 = (s32[]{:T(128)}, f32[2,64,128]{2,1,0:T(8,128)S(1)}, f32[2,64]{1,0:T(2,128)S(1)}, f32[12,2,64,128]{3,2,0,1:T(8,128)S(1)}, f32[12,2,64,64]{3,2,1,0:T(8...) while((s32[]{:T(128)}, f32[2,64,128]{2,1,0:T(8,128)S(1)}, ...), condition=%wide.region_7.8_spmd.clone, body=%wide.region_5.7_spmd.clone.sunk | while | flops 41005312 | bytes 9845901 | solution.py:75
  211.1 5.6 copy.197
  228.6 5.6 copy.197
  246.0 5.6 copy.197
  263.4 5.6 copy.197
  280.8 5.6 copy.197
  298.3 5.6 copy.197
  315.7 5.6 copy.197
  333.1 5.6 copy.197
  350.6 5.6 copy.197
  368.0 5.6 copy.197
  385.4 5.6 copy.197
  402.8 5.6 copy.197
  420.2 12.8 %all-gather.6 = bf16[4,2,64]{2,1,0:T(2,128)(2,1)S(1)} all-gather(bf16[1,2,64]{2,1,0:T(2,128)(2,1)S(1)} %fusion.66), channel_id=4, replica_groups=mesh['grp'=2,'sp'=4,'tp'=4] {'sp'}, dimensions={0}, use_global_device_ids=true | all-gather | bytes 1280 | tf_op jit(solution)/shard_map/all_gather | solution.py:18
  433.0 13.4 %all-gather.3 = bf16[8,64,128]{2,1,0:T(8,128)(2,1)S(1)} all-gather(bf16[2,64,128]{2,1,0:T(8,128)(2,1)S(1)} %convert_element_type.105), channel_id=5, replica_groups=mesh['grp'=2,'sp'=4,'tp'=4] {'sp'}, dimensions={0}, use_global_device_ids=true | all-gather | bytes 163840 | tf_op jit(solution)/shard_map/all_gather | solution.py:18
  448.7 7.3 %rev.19 = f32[768,2,128]{0,2,1:T(8,128)} reverse(f32[768,2,128]{0,2,1:T(8,128)} %fusion.48), dimensions={0} | reverse | bytes 1572864 | tf_op jit(solution)/shard_map/rev | solution.py:176
  458.2 7.6 %all-gather.5 = bf16[4,2,64]{2,1,0:T(2,128)(2,1)S(1)} all-gather(bf16[1,2,64]{2,1,0:T(2,128)(2,1)S(1)} %fusion.65), channel_id=2, replica_groups=mesh['grp'=2,'sp'=4,'tp'=4] {'sp'}, dimensions={0}, use_global_device_ids=true | all-gather | bytes 1280 | tf_op jit(solution)/shard_map/all_gather | solution.py:18
  465.8 13.3 %all-gather.1 = bf16[8,64,128]{2,1,0:T(8,128)(2,1)S(1)} all-gather(bf16[2,64,128]{2,1,0:T(8,128)(2,1)S(1)} %convert_element_type.103), channel_id=3, replica_groups=mesh['grp'=2,'sp'=4,'tp'=4] {'sp'}, dimensions={0}, use_global_device_ids=true | all-gather | bytes 163840 | tf_op jit(solution)/shard_map/all_gather | solution.py:18
  482.2 9.9 %all_to_all.16 = bf16[4,192,256]{2,1,0:T(8,128)(2,1)S(1)} all-to-all(bf16[4,192,256]{2,1,0:T(8,128)(2,1)S(1)} %convert_element_type.107), channel_id=1, replica_groups=mesh['grp'=2,'sp'=4,'tp'=4] {'tp'}, dimensions={0} | all-to-all | bytes 786432 | tf_op jit(solution)/shard_map/all_to_all | solution.py:177
  492.2 3.5 multiply_reduce_fusion
  497.5 8.0 %copy.121 = bf16[1280,4,512]{0,2,1:T(8,128)(2,1)} copy(bf16[1280,4,512]{2,0,1:T(8,128)(2,1)} %bitcast.244) | data formatting | bytes 10485760 | tf_op jit(solution)/shard_map/reshape | solution.py:185
  505.5 19.2 %all-gather.15.cloned.1.call-done = bf16[768,2048]{1,0:T(8,128)(2,1)} async-done(((bf16[192,2048]{1,0:T(8,128)(2,1)}), bf16[768,2048]{1,0:T(8,128)(2,1)}) %all-gather.15.cloned.1.call-update) | async-done | bytes 3145744 | tf_op jit(solution)/shard_map/all_gather | solution.py:188
  524.7 9.6 %fusion.70 = f32[768,1280]{1,0:T(8,128)} fusion(bf16[768,2048]{1,0:T(8,128)(2,1)} %all-gather.15.cloned.1.call-done, bf16[2048,1280]{1,0:T(8,128)(2,1)} %all-gather.17.cloned.1.call-done), kind=kOutput, calls=%fused_computation.119 | convolution fusion | flops 4026531840 | bytes 12320768 | tf_op jit(solution)/shard_map/dot_general | solution.py:189
  534.3 89.9 %all-gather.19.cloned.1.call-done = bf16[2048,1280]{1,0:T(8,128)(2,1)} async-done(((bf16[512,1280]{1,0:T(8,128)(2,1)}), bf16[2048,1280]{1,0:T(8,128)(2,1)}) %all-gather.19.cloned.1.call-update) | async-done | bytes 5242896 | tf_op jit(solution)/shard_map/all_gather | solution.py:184
  624.2 16.0 %convolution_convert_fusion = bf16[768,2048]{1,0:T(8,128)(2,1)} fusion(bf16[1280,2048]{0,1:T(8,128)(2,1)} %bitcast.245, bf16[768,2048]{1,0:T(8,128)(2,1)} %all-gather.15.cloned.1.call-done, bf16[2048,1280]{1,0:T(8,128)(2,1)} %all-gather.19.cloned.1.call-done, f32[768,1280]{1,0:T(8,128)} %fusion.70), kind=kOutput, calls=%fused_computation.75 | convolution fusion | flops 8060534784 | bytes 20709376 | tf_op jit(solution)/shard_map/dot_general | solution.py:193
  640.2 36.4 %reduce-scatter.2.cloned.1.call-done = bf16[192,2048]{1,0:T(8,128)(2,1)} async-done(((bf16[768,2048]{1,0:T(8,128)(2,1)}), bf16[192,2048]{1,0:T(8,128)(2,1)}) %reduce-scatter.2.cloned.1.call-update) | async-done | bytes 786448 | tf_op jit(solution)/shard_map/reduce_scatter | solution.py:192
  (466 shorter events, 261.4 us)
Async XLA Ops:
  6.5 3.7 copy-start.3
  6.5 485.7 %all-gather.13.cloned.1.call-start = ((), (), s32[]{:S(2)}) async-start(), calls=%async_computation.2 | async-start | bytes 5242880 | tf_op jit(solution)/shard_map/all_gather | solution.py:178
  6.5 5.5 copy-start.9
  6.5 5.6 copy-start.4
  6.5 5.8 copy-start.6
  7.3 490.3 %all-gather.21.cloned.1.call-start = ((), (), s32[]{:S(2)}) async-start(), calls=%async_computation.7 | async-start | bytes 6553600 | tf_op jit(solution)/shard_map/all_gather | solution.py:185
  8.0 497.5 %all-gather.17.cloned.1.call-start = ((), (), s32[]{:S(2)}) async-start(), calls=%async_computation.4 | async-start | bytes 6553600 | tf_op jit(solution)/shard_map/all_gather | solution.py:183
  8.7 515.9 %all-gather.15.cloned.1.call-start = ((), (), s32[]{:S(2)}) async-start(), calls=%async_computation.3 | async-start | bytes 3932160 | tf_op jit(solution)/shard_map/all_gather | solution.py:188
  12.5 8.5 %copy-start.5 = (bf16[768,128]{1,0:T(8,128)(2,1)S(1)}, bf16[768,128]{1,0:T(8,128)(2,1)}, u32[]{:S(2)}) copy-start(bf16[768,128]{1,0:T(8,128)(2,1)} %param.23) | copy-start | bytes 589828
  416.0 0.9 copy-start
  448.7 9.3 %copy-start.2 = (bf16[768,256]{1,0:T(8,128)(2,1)S(1)}, bf16[768,256]{1,0:T(8,128)(2,1)}, u32[]{:S(2)}) copy-start(bf16[768,256]{1,0:T(8,128)(2,1)} %param.26) | copy-start | bytes 1179652
  456.5 22.6 %copy-start.1 = (f32[768,2,128]{0,2,1:T(8,128)S(1)}, f32[768,2,128]{0,2,1:T(8,128)}, u32[]{:S(2)}) copy-start(f32[768,2,128]{0,2,1:T(8,128)} %rev.19) | copy-start | bytes 2359300
  456.5 24.6 %copy-start.8 = (f32[256]{0:T(256)S(1)}, f32[256]{0:T(256)}, u32[]{:S(2)}) copy-start(f32[256]{0:T(256)} %param.32) | copy-start | bytes 3076
  482.2 13.6 %copy-start.7 = (f32[2048]{0:T(1024)S(1)}, f32[2048]{0:T(1024)}, u32[]{:S(2)}) copy-start(f32[2048]{0:T(1024)} %param.34) | copy-start | bytes 24580
  496.9 127.3 %all-gather.19.cloned.1.call-start = ((), (), s32[]{:S(2)}) async-start(), calls=%async_computation.5 | async-start | bytes 6553600 | tf_op jit(solution)/shard_map/all_gather | solution.py:184
  497.5 179.1 %reduce-scatter.2.cloned.1.call-start = ((), (), s32[]{:S(2)}) async-start(), calls=%async_computation.6 | async-start | bytes 3932160 | tf_op jit(solution)/shard_map/reduce_scatter | solution.py:192
Sparse Core Ops, SparseCore 0:
  8.9 37.2 all-gather.12
  47.7 97.9 all-gather.20
  147.3 96.3 all-gather.16
  497.0 27.6 all-gather.14
  526.1 98.0 all-gather.18
  640.3 36.1 reduce-scatter.1
